TPU v7x, 32 devices: a whole 2x2x4 slice. The times are simulated.
32 devices in a mesh: sp: 16 (over z, y, x), tp: 2 (over core).
Axes of the slice: x: 2, y: 2, z: 4, core: 2. Of those that a mesh axis runs over, the one named last changes fastest.
Arguments:
- latent: bfloat16 [4096, 2048], P(('sp', 'tp')), may hold values from -3 to 3
- context: bfloat16 [1024, 2048], P('sp'), may hold values from -6 to 6
- condition: float32 [2048], replicated, may hold values from -6 to 6
- ctx_cond: float32 [2048], replicated, may hold values from -6 to 6
- norm_gain: float32 [2048], replicated, may hold values from 0.1 to 1.9
- w_shift: bfloat16 [2048, 2048], P('sp', 'tp'), may hold values from -0.25 to 0.25
- w_scale: bfloat16 [2048, 2048], P('sp', 'tp'), may hold values from -0.25 to 0.25
- w_gate: bfloat16 [2048, 2048], P('sp', 'tp'), may hold values from -0.25 to 0.25
- w_query: bfloat16 [2048, 2048], P(None, 'tp'), may hold values from -0.125 to 0.125
- w_key: bfloat16 [2048, 2048], P(None, 'tp'), may hold values from -0.125 to 0.125
- w_value: bfloat16 [2048, 2048], P(None, 'tp'), may hold values from -0.125 to 0.125
- w_out: bfloat16 [2048, 2048], P('tp'), may hold values from -0.125 to 0.125
- rel_bias: float32 [16, 15, 31], replicated, may hold values from 2 to 250
Outputs:
- updated: bfloat16 [4096, 2048], P(('sp', 'tp'))
All inputs are finite; a program needn't handle non-finite values.
Results may differ from a plain program's by a relative error of at most 0.015.
Values may be sent and summed in bfloat16 or wider, within the bound.
A program may use at most 128 MiB of HBM per device.

v0:
```python
import jax
import jax.numpy as jnp
from jax import lax
from jax.sharding import PartitionSpec as P

HEADS = 16
HEAD_DIM = 128
GRID_W = 32
WIN_H = 8
WIN_W = 16
NORM_EPS = 1e-06
NEG_BIG = -1e30


def padded_2(cells, sides, width):
    for axis, dim in sides:
        count = lax.axis_size(axis)
        ends = count - 1
        head = lax.slice_in_dim(cells, 0, width, axis=dim)
        tail = lax.slice_in_dim(cells, cells.shape[dim] - width, cells.shape[dim], axis=dim)
        cells = jnp.concatenate(
            [
                lax.ppermute(tail, axis, [(i, (i + 1) % count) for i in range(ends)]),
                cells,
                lax.ppermute(head, axis, [((i + 1) % count, i) for i in range(ends)]),
            ],
            axis=dim,
        )
    return cells


def rms_mod(block, norm_gain, shifts, scales):
    block = block.astype(jnp.float32)
    normed = (
        block * lax.rsqrt(jnp.mean(block * block, axis=-1, keepdims=True) + NORM_EPS) * norm_gain
    )
    return (normed * (1.0 + scales) + shifts).astype(jnp.bfloat16)


def project(block, weights):
    return jnp.stack(
        [
            jnp.dot(block, weight, preferred_element_type=jnp.float32).astype(jnp.bfloat16)
            for weight in weights
        ]
    )


def on_device(
    latent,
    context,
    condition,
    ctx_cond,
    norm_gain,
    w_shift,
    w_scale,
    w_gate,
    w_query,
    w_key,
    w_value,
    w_out,
    rel_bias,
):
    tp_size = lax.axis_size("tp")
    sp_size = lax.axis_size("sp")
    head_dev = HEADS // tp_size
    head_cols = w_query.shape[1]
    model_width = w_query.shape[0]
    row_part = w_shift.shape[0]
    col_part = w_shift.shape[1]
    activated = jax.nn.silu(jnp.stack([condition, ctx_cond])).astype(jnp.bfloat16)
    act_rows = lax.dynamic_slice_in_dim(activated, lax.axis_index("sp") * row_part, row_part, 1)
    partial_value = jnp.concatenate(
        [
            jnp.dot(act_rows, w_shift, preferred_element_type=jnp.float32),
            jnp.dot(act_rows, w_scale, preferred_element_type=jnp.float32),
            jnp.dot(act_rows[:1], w_gate, preferred_element_type=jnp.float32),
        ],
        axis=0,
    )
    placed = lax.dynamic_update_slice_in_dim(
        jnp.zeros((5, model_width), jnp.float32), partial_value, lax.axis_index("tp") * col_part, 1
    )
    mod_vecs = lax.psum(placed, ("sp", "tp"))
    normed = rms_mod(latent, norm_gain, mod_vecs[0], mod_vecs[2])
    projected = project(lax.all_gather(normed, "tp", axis=0, tiled=True), (w_query, w_key, w_value))
    ctx_kv = lax.all_gather(
        project(rms_mod(context, norm_gain, mod_vecs[1], mod_vecs[3]), (w_key, w_value)),
        "sp",
        axis=1,
        tiled=True,
    )
    ctx_key3 = ctx_kv[0].reshape(-1, head_dev, HEAD_DIM)
    ctx_val3 = ctx_kv[1].reshape(-1, head_dev, HEAD_DIM)
    grid_rows = projected.shape[1] // GRID_W
    queries = projected[0].reshape(grid_rows, GRID_W, head_dev, HEAD_DIM)
    half_win = WIN_H // 2
    padded = padded_2(
        projected[1:].reshape(2, grid_rows, GRID_W, head_cols), (("sp", 1),), half_win
    )
    total_rows = grid_rows * sp_size
    first_row = lax.axis_index("sp") * grid_rows
    local_rows = jnp.arange(grid_rows, dtype=jnp.int32)
    starts = (
        jnp.clip(first_row + local_rows - half_win, 0, total_rows - WIN_H) - first_row + half_win
    )

    def take_window(start_row):
        return lax.dynamic_slice_in_dim(padded, start_row, WIN_H, 1)

    windows = jax.vmap(take_window)(starts)
    key_win = windows[:, 0].reshape(grid_rows, WIN_H, GRID_W, head_dev, HEAD_DIM)
    val_win = windows[:, 1].reshape(grid_rows, WIN_H, GRID_W, head_dev, HEAD_DIM)
    row_off = (
        starts[:, None]
        - half_win
        + jnp.arange(WIN_H, dtype=jnp.int32)[None, :]
        - local_rows[:, None]
        + WIN_H
        - 1
    )
    col_ids = jnp.arange(GRID_W, dtype=jnp.int32)
    col_start = jnp.clip(col_ids - WIN_W // 2, 0, GRID_W - WIN_W)
    col_in = (col_ids[None, :] >= col_start[:, None]) & (
        col_ids[None, :] < col_start[:, None] + WIN_W
    )
    col_off = jnp.clip(col_ids[None, :] - col_ids[:, None], 1 - WIN_W, WIN_W - 1) + WIN_W - 1
    col_hot = (col_off[:, :, None] == jnp.arange(2 * WIN_W - 1)[None, None, :]).astype(jnp.float32)
    row_hot = (row_off[:, :, None] == jnp.arange(2 * WIN_H - 1)[None, None, :]).astype(jnp.float32)
    bias_table = lax.dynamic_slice_in_dim(rel_bias, lax.axis_index("tp") * head_dev, head_dev, 0)
    col_table = jnp.einsum("hec,qwc->heqw", bias_table, col_hot, precision=lax.Precision.HIGHEST)
    bias_win = jnp.einsum("rke,heqw->rqhkw", row_hot, col_table, precision=lax.Precision.HIGHEST)
    inv_scale = HEAD_DIM ** (-0.5)
    scores_win = (
        jnp.einsum("rqhd,rkwhd->rqhkw", queries, key_win, preferred_element_type=jnp.float32)
        * inv_scale
        + bias_win
    )
    scores_win = jnp.where(col_in[None, :, None, None, :], scores_win, NEG_BIG)
    scores_win = scores_win.reshape(grid_rows, GRID_W, head_dev, WIN_H * GRID_W)
    scores_ctx = (
        jnp.einsum("rqhd,chd->rqhc", queries, ctx_key3, preferred_element_type=jnp.float32)
        * inv_scale
    )
    row_max = jnp.maximum(jnp.max(scores_win, axis=-1), jnp.max(scores_ctx, axis=-1))
    exp_win = jnp.exp(scores_win - row_max[..., None])
    exp_ctx = jnp.exp(scores_ctx - row_max[..., None])
    row_total = jnp.sum(exp_win, axis=-1) + jnp.sum(exp_ctx, axis=-1)
    probs_win = (exp_win / row_total[..., None]).astype(jnp.bfloat16)
    probs_win = probs_win.reshape(grid_rows, GRID_W, head_dev, WIN_H, GRID_W)
    probs_ctx = (exp_ctx / row_total[..., None]).astype(jnp.bfloat16)
    attended = jnp.einsum(
        "rqhkw,rkwhd->rqhd", probs_win, val_win, preferred_element_type=jnp.float32
    )
    attended = attended + jnp.einsum(
        "rqhc,chd->rqhd", probs_ctx, ctx_val3, preferred_element_type=jnp.float32
    )
    attended = attended.astype(jnp.bfloat16).reshape(grid_rows * GRID_W, head_cols)
    branch = lax.psum_scatter(
        jnp.dot(attended, w_out, preferred_element_type=jnp.float32).astype(jnp.bfloat16),
        "tp",
        scatter_dimension=0,
        tiled=True,
    ).astype(jnp.float32)
    return (latent.astype(jnp.float32) + mod_vecs[4] * branch).astype(jnp.bfloat16)


def solution(mesh):
    placed = (
        P(("sp", "tp"), None),
        P("sp", None),
        P(),
        P(),
        P(),
        P("sp", "tp"),
        P("sp", "tp"),
        P("sp", "tp"),
        P(None, "tp"),
        P(None, "tp"),
        P(None, "tp"),
        P("tp", None),
        P(),
    )
    return jax.shard_map(
        on_device, mesh=mesh, in_specs=placed, out_specs=P(("sp", "tp"), None), check_vma=False
    )
```

profile of v0, /device:TPU:0, one launch (start us, length us, event | category | flops | bytes accessed | tf_op | source)
XLA Modules:
  0.0 193.7 jit_solution(12751256618278326930)
XLA Ops:
  9.9 42.3 %psum.7 = f32[5,2048]{1,0:T(8,128)S(1)} all-reduce(f32[5,2048]{1,0:T(8,128)S(1)} %maximum_dynamic-update-slice_fusion), channel_id=1, replica_groups=mesh['sp'=16,'tp'=2] {'sp','tp'}, use_global_device_ids=true, to_apply=%region_0.1 | all-reduce | flops 10240 | bytes 81920 | tf_op jit(solution)/shard_map/psum | solution.py:84
  53.5 2.1 %fusion.39 = bf16[128,2048]{1,0:T(8,128)(2,1)} fusion(bf16[128,2048]{1,0:T(8,128)(2,1)} %param.13, f32[2048]{0:T(1024)S(1)} %bitcast.155, f32[2048]{0:T(1024)S(1)} %bitcast.156, f32[2048]{0:T(1024)} %param.17, f32[128]{0:T(128)S(1)} %add_rsqrt_fusion.1), kind=kLoop, calls=%fused_computation.46 | loop fusion | flops 1572864 | bytes 1073664 | tf_op jit(solution)/shard_map/convert_element_type | solution.py:37
  57.0 3.2 %fusion.33 = bf16[1,64,1024]{2,1,0:T(8,128)(2,1)S(1)} fusion(bf16[2048,1024]{1,0:T(8,128)(2,1)} %param.22, bf16[64,2048]{1,0:T(8,128)(2,1)} %param.14, f32[2048]{0:T(1024)S(1)} %bitcast.150, f32[2048]{0:T(1024)S(1)} %bitcast.152, f32[2048]{0:T(1024)} %param.17, f32[64]{0:T(128)S(1)} %add_rsqrt_fusion), kind=kOutput, calls=%fused_computation.40 | convolution fusion | flops 269287424 | bytes 4612352 | tf_op jit(solution)/shard_map/dot_general | solution.py:43
  62.1 1.4 fusion.51
  63.5 5.6 %fusion.12 = f32[8,32,32,8,8]{2,4,3,1,0:T(8,128)} fusion(f32[8,15,32,32]{3,1,2,0:T(8,128)S(1)} %fusion.51, s32[8,8]{1,0:T(8,128)S(1)} %subtract_add_fusion), kind=kOutput, calls=%fused_computation.21 | convolution fusion | flops 94372800 | bytes 2588928 | tf_op jit(solution)/shard_map/rke,heqw->rqhkw/dot_general | solution.py:132
  69.2 9.3 %copy.59 = f32[8,32,32,8,8]{1,2,4,0,3:T(8,128)} copy(f32[8,32,32,8,8]{2,4,3,1,0:T(8,128)} %fusion.12) | data formatting | bytes 4194304 | tf_op jit(solution)/shard_map/rke,heqw->rqhkw/dot_general | solution.py:132
  78.5 3.9 %convolution_convert_fusion.2 = bf16[256,1024]{1,0:T(8,128)(2,1)S(1)} fusion(bf16[256,2048]{1,0:T(8,128)(2,1)} %all-gather.3.cloned.1.call-done, bf16[2048,1024]{1,0:T(8,128)(2,1)} %param.23), kind=kOutput, calls=%fused_computation.35 | convolution fusion | flops 1074003968 | bytes 5767168 | tf_op jit(solution)/shard_map/dot_general | solution.py:43
  83.9 4.2 %collective-permute-start = (bf16[2,4,32,1024]{3,2,0,1:T(8,128)(2,1)S(1)}, bf16[2,4,32,1024]{3,2,0,1:T(8,128)(2,1)S(1)}, u32[]{:S(2)}, u32[]{:S(2)}) collective-permute-start(bf16[2,4,32,1024]{3,2,0,1:T(8,128)(2,1)S(1)} %get-tuple-element.9), channel_id=1, source_target_pairs={{0,2},{2,4},{4,6},{6,8},{8,10},{10,12},{12,14},{14,16},{16,18},{18... | collective-permute-start | bytes 1572872 | tf_op jit(solution)/shard_map/ppermute | solution.py:23
  88.2 1.3 collective-permute-start.1
  91.0 25.2 %collective-permute-done = bf16[2,4,32,1024]{3,2,0,1:T(8,128)(2,1)S(1)} collective-permute-done((bf16[2,4,32,1024]{3,2,0,1:T(8,128)(2,1)S(1)}, bf16[2,4,32,1024]{3,2,0,1:T(8,128)(2,1)S(1)}, u32[]{:S(2)}, u32[]{:S(2)}) %collective-permute-start) | collective-permute-done | bytes 524320 | tf_op jit(solution)/shard_map/ppermute | solution.py:23
  116.2 1.9 collective-permute-done.1
  118.4 4.9 %gather_fusion = bf16[8,2,8,32,1024]{4,3,1,2,0:T(8,128)(2,1)} fusion(bf16[2,16,32,1024]{3,2,0,1:T(8,128)(2,1)S(1)} %pad_maximum_fusion, s32[8]{0:T(128)S(1)} %shift-left_bitcast_fusion), kind=kCustom, calls=%fused_computation | custom fusion | bytes 16777344 | tf_op jit(solution)/shard_map/vmap()/gather | solution.py:109
  123.3 4.0 %fusion.66 = (bf16[8,1,8,32,1024]{4,3,1,2,0:T(8,128)(2,1)S(1)}, bf16[8,1,8,32,1024]{4,3,1,2,0:T(8,128)(2,1)S(1)}) fusion(bf16[8,2,8,32,1024]{4,3,1,2,0:T(8,128)(2,1)} %gather_fusion), kind=kLoop, calls=%fused_computation.99 | loop fusion | bytes 16777216 | tf_op jit(solution)/shard_map/slice | solution.py:113
  128.4 3.3 %copy.80 = bf16[256,8,8,128]{3,2,1,0:T(8,128)(2,1)} copy(bf16[256,8,8,128]{3,1,2,0:T(8,128)(2,1)S(1)} %bitcast.137) | data formatting | bytes 8388608
  132.9 4.3 %fusion.68 = (f32[8,32,8]{1,2,0:T(8,128)S(1)}, f32[8,32,8,8,32]{1,4,3,2,0:T(8,128)}) fusion(f32[8,32,32,8,8]{1,2,4,0,3:T(8,128)S(1)} %bitcast.133, bf16[8,32,8,128,1]{3,2,1,0,4:T(8,128)(2,1)S(1)} %bitcast_bitcast_fusion, bf16[8,8,32,8,128]{4,3,2,1,0:T(8,128)(2,1)S(1)} %bitcast.136, pred[32,32]{0,1:T(8,128)(4,1)S(1)} %fusion.57), kind=kOutput, calls=%fused_computation.101 | convolution fusion | flops 136312832 | bytes 8922112 | tf_op jit(solution)/shard_map/rqhd,rkwhd->rqhkw/dot_general | solution.py:135
  137.2 19.0 %all-gather.5.cloned.1.call-done = bf16[2,1024,1024]{2,1,0:T(8,128)(2,1)} async-done(((bf16[2,64,1024]{2,1,0:T(8,128)(2,1)}), bf16[2,1024,1024]{2,1,0:T(8,128)(2,1)}) %all-gather.5.cloned.1.call-update) | async-done | bytes 4194320 | tf_op jit(solution)/shard_map/all_gather | solution.py:87
  156.2 3.2 %slice_bitcast_fusion = (bf16[128,8,8,128]{3,1,2,0:T(8,128)(2,1)S(1)}, bf16[128,8,8,128]{3,1,2,0:T(8,128)(2,1)S(1)}) fusion(bf16[2,1024,1024]{2,1,0:T(8,128)(2,1)} %all-gather.5.cloned.1.call-done), kind=kLoop, calls=%fused_computation.18 | loop fusion | bytes 8388608
  162.0 1.9 fusion.3
  164.9 2.0 %fusion.2 = f32[8,32,8]{1,2,0:T(8,128)S(1)} fusion(f32[8,32,8,8,32]{1,4,3,2,0:T(8,128)S(1)} %bitcast.135, f32[8,32,8]{1,2,0:T(8,128)S(1)} %copy_maximum_fusion), kind=kLoop, calls=%fused_computation.9 | loop fusion | flops 1046528 | bytes 2113536 | tf_op jit(solution)/shard_map/reduce_sum | solution.py:148
  167.6 3.3 %fusion.21 = f32[8,32,8,128]{3,1,2,0:T(8,128)S(1)} fusion(bf16[1024,8,128]{2,1,0:T(8,128)(2,1)S(1)} %bitcast.143, f32[8,32,8]{1,0,2:T(8,128)S(1)} %copy.67, f32[8,32,8]{1,0,2:T(8,128)S(1)} %copy.63, f32[8,1024,256]{1,2,0:S(1)} %fusion.16), kind=kOutput, calls=%fused_computation.31 | convolution fusion | flops 545259520 | bytes 11550720 | tf_op jit(solution)/shard_map/rqhc,chd->rqhd/dot_general | solution.py:155
  170.9 2.3 %fusion.29 = bf16[8,32,8,128]{3,1,2,0:T(8,128)(2,1)S(1)} fusion(f32[8,32,8,128]{3,1,2,0:T(8,128)S(1)} %fusion.21, f32[8,32,8,8,32]{1,4,3,2,0:T(8,128)S(1)} %bitcast.135, f32[8,32,8]{1,2,0:T(8,128)S(1)} %copy_add_fusion, f32[8,32,8]{1,2,0:T(8,128)S(1)} %copy_maximum_fusion, bf16[8,8,32,8,128]{4,3,2,1,0:T(8,128)(2,1)S(1)} %bitcast.142), kind=kOutput, calls=%fused_computation.33 | convolution fusion | flops 136314880 | bytes 7880704 | tf_op jit(solution)/shard_map/rqhkw,rkwhd->rqhd/dot_general | solution.py:152
  173.5 4.5 %convolution_convert_fusion = bf16[256,2048]{1,0:T(8,128)(2,1)} fusion(bf16[1024,2048]{1,0:T(8,128)(2,1)} %param.24, bf16[32,8,8,128]{3,2,1,0:T(8,128)(2,1)S(1)} %bitcast.149), kind=kOutput, calls=%fused_computation.17 | convolution fusion | flops 1074266112 | bytes 5767168 | tf_op jit(solution)/shard_map/dot_general | solution.py:160
  178.0 7.1 %reduce-scatter.2.cloned.1.call-done = bf16[128,2048]{1,0:T(8,128)(2,1)} async-done(((bf16[256,2048]{1,0:T(8,128)(2,1)}), bf16[128,2048]{1,0:T(8,128)(2,1)}) %reduce-scatter.2.cloned.1.call-update) | async-done | bytes 524304 | tf_op jit(solution)/shard_map/reduce_scatter | solution.py:159
  185.1 2.0 %fusion.40 = bf16[128,2048]{1,0:T(8,128)(2,1)} fusion(bf16[128,2048]{1,0:T(8,128)(2,1)S(1)} %copy-done.2, bf16[128,2048]{1,0:T(8,128)(2,1)} %reduce-scatter.2.cloned.1.call-done, f32[2048]{0:T(1024)S(1)} %bitcast.154), kind=kLoop, calls=%fused_computation.47 | loop fusion | flops 1310720 | bytes 1581056 | tf_op jit(solution)/shard_map/convert_element_type | solution.py:165
  (76 shorter events, 17.9 us)
Async XLA Ops:
  6.5 1.0 copy-start
  6.5 53.7 %copy-start.7 = (f32[2048]{0:T(1024)S(1)}, f32[2048]{0:T(1024)}, u32[]{:S(2)}) copy-start(f32[2048]{0:T(1024)} %param.17) | copy-start | bytes 24580
  6.5 53.7 %copy-start.6 = (bf16[64,2048]{1,0:T(8,128)(2,1)S(1)}, bf16[64,2048]{1,0:T(8,128)(2,1)}, u32[]{:S(2)}) copy-start(bf16[64,2048]{1,0:T(8,128)(2,1)} %param.14) | copy-start | bytes 786436
  6.5 72.0 %all-gather.3.cloned.1.call-start = ((), (), s32[]{:S(2)}) async-start(), calls=%async_computation.1 | async-start | bytes 1572864 | tf_op jit(solution)/shard_map/all_gather | solution.py:86
  55.6 100.6 %all-gather.5.cloned.1.call-start = ((), (), s32[]{:S(2)}) async-start(), calls=%async_computation.2 | async-start | bytes 4456448 | tf_op jit(solution)/shard_map/all_gather | solution.py:87
  55.7 4.6 %copy-start.3 = (bf16[2048,1024]{1,0:T(8,128)(2,1)S(1)}, bf16[2048,1024]{1,0:T(8,128)(2,1)}, u32[]{:S(2)}) copy-start(bf16[2048,1024]{1,0:T(8,128)(2,1)} %param.23) | copy-start | bytes 12582916
  56.9 5.0 %copy-start.8 = (f32[16,15,31]{2,0,1:T(8,128)S(1)}, f32[16,15,31]{2,0,1:T(8,128)}, u32[]{:S(2)}) copy-start(f32[16,15,31]{2,0,1:T(8,128)} %param.25) | copy-start | bytes 89284
  61.9 123.2 %reduce-scatter.2.cloned.1.call-start = ((), (), s32[]{:S(2)}) async-start(), calls=%async_computation.3 | async-start | bytes 1572864 | tf_op jit(solution)/shard_map/reduce_scatter | solution.py:159
  78.5 3.9 %copy-start.4 = (bf16[2048,1024]{1,0:T(8,128)(2,1)S(1)}, bf16[2048,1024]{1,0:T(8,128)(2,1)}, u32[]{:S(2)}) copy-start(bf16[2048,1024]{1,0:T(8,128)(2,1)} %param.22) | copy-start | bytes 12582916
  78.5 4.0 %copy-start.10 = (bf16[256,2048]{1,0:T(8,128)(2,1)S(1)}, bf16[256,2048]{1,0:T(8,128)(2,1)}, u32[]{:S(2)}) copy-start(bf16[256,2048]{1,0:T(8,128)(2,1)} %all-gather.3.cloned.1.call-done) | copy-start | bytes 3145732
  82.6 6.9 %copy-start.9 = (bf16[2048,1024]{1,0:T(8,128)(2,1)S(1)}, bf16[2048,1024]{1,0:T(8,128)(2,1)}, u32[]{:S(2)}) copy-start(bf16[2048,1024]{1,0:T(8,128)(2,1)} %param.21) | copy-start | bytes 12582916
  83.9 32.3 %collective-permute-start = (bf16[2,4,32,1024]{3,2,0,1:T(8,128)(2,1)S(1)}, bf16[2,4,32,1024]{3,2,0,1:T(8,128)(2,1)S(1)}, u32[]{:S(2)}, u32[]{:S(2)}) collective-permute-start(bf16[2,4,32,1024]{3,2,0,1:T(8,128)(2,1)S(1)} %get-tuple-element.9), channel_id=1, source_target_pairs={{0,2},{2,4},{4,6},{6,8},{8,10},{10,12},{12,14},{14,16},{16,18},{18... | collective-permute-start | bytes 1572872 | tf_op jit(solution)/shard_map/ppermute | solution.py:23
  88.2 30.0 %collective-permute-start.1 = (bf16[2,4,32,1024]{3,2,0,1:T(8,128)(2,1)S(1)}, bf16[2,4,32,1024]{3,2,0,1:T(8,128)(2,1)S(1)}, u32[]{:S(2)}, u32[]{:S(2)}) collective-permute-start(bf16[2,4,32,1024]{3,2,0,1:T(8,128)(2,1)S(1)} %get-tuple-element.10), channel_id=1, source_target_pairs={{2,0},{4,2},{6,4},{8,6},{10,8},{12,10},{14,12},{16,14},{18,16},{20... | collective-permute-start | bytes 1572872 | tf_op jit(solution)/shard_map/ppermute | solution.py:25
  127.3 4.5 %slice-start = ((s8[8388608]{0:T(1024)(128)(4,1)}), s8[4194304]{0:T(1024)(128)(4,1)S(1)}, s32[]{:S(2)}) async-start(s8[8388608]{0:T(1024)(128)(4,1)} %bitcast.132), calls=%async_computation.4 | async-start | bytes 8388608
  128.4 4.5 %slice-start.1 = ((s8[8388608]{0:T(1024)(128)(4,1)}), s8[4194304]{0:T(1024)(128)(4,1)S(1)}, s32[]{:S(2)}) async-start(s8[8388608]{0:T(1024)(128)(4,1)} %bitcast.132), calls=%async_computation.5 | async-start | bytes 8388608
  161.3 2.6 %slice-start.2 = ((s8[8388608]{0:T(1024)(128)(4,1)}), s8[4194304]{0:T(1024)(128)(4,1)S(1)}, s32[]{:S(2)}) async-start(s8[8388608]{0:T(1024)(128)(4,1)} %bitcast.134), calls=%async_computation.6 | async-start | bytes 8388608
  162.0 2.9 %slice-start.3 = ((s8[8388608]{0:T(1024)(128)(4,1)}), s8[4194304]{0:T(1024)(128)(4,1)S(1)}, s32[]{:S(2)}) async-start(s8[8388608]{0:T(1024)(128)(4,1)} %bitcast.134), calls=%async_computation.7 | async-start | bytes 8388608
  167.6 3.3 %copy-start.5 = (bf16[256,8,8,128]{3,2,1,0:T(8,128)(2,1)S(1)}, bf16[256,8,8,128]{3,2,1,0:T(8,128)(2,1)}, u32[]{:S(2)}) copy-start(bf16[256,8,8,128]{3,2,1,0:T(8,128)(2,1)} %copy.80) | copy-start | bytes 12582916
  173.5 11.7 %copy-start.2 = (bf16[128,2048]{1,0:T(8,128)(2,1)S(1)}, bf16[128,2048]{1,0:T(8,128)(2,1)}, u32[]{:S(2)}) copy-start(bf16[128,2048]{1,0:T(8,128)(2,1)} %param.13) | copy-start | bytes 1572868
  173.5 13.6 %copy-start.1 = (bf16[128,1024]{1,0:T(8,128)(2,1)S(1)}, bf16[128,1024]{1,0:T(8,128)(2,1)}, u32[]{:S(2)}) copy-start(bf16[128,1024]{1,0:T(8,128)(2,1)} %param.18) | copy-start | bytes 786436
Sparse Core Ops, SparseCore 0:
  55.7 8.8 all-gather.2
  67.3 88.8 all-gather.4
  178.1 6.9 reduce-scatter.1
where the time goes:
time: 194 us
  waiting for transfers between devices  53.3 us (27%)
  blocking collectives  42.3 us (22%)
  matrix products  35.6 us (18%)
  local copies, waits for them, and re-layouts  30 us (15%)
  between operations  13.6 us (7%)
  other arithmetic  13.3 us (7%)
  starting transfers between devices  5.61 us (3%)
    psum x1, blocking collectives, on_device(): mod_vecs = lax.psum(placed, ('sp', 'tp'))  42.3 us
    ppermute x1, waiting for transfers between devices, padded_2(): lax.ppermute(tail, axis, [(i, (i + 1) % count) for i in range(ends)])  25.2 us
    all_gather x1, waiting for transfers between devices, on_device(): lax.all_gather(project(rms_mod(context, norm_gain, mod_vecs[1], mod_vecs[...  19 us
    unnamed x36, local copies, waits for them, and re-layouts  11.5 us
    dot_general x5, matrix products, project(): jnp.dot(block, weight, preferred_element_type=jnp.float32)  10.6 us
    dot_general x1, local copies, waits for them, and re-layouts, on_device(): jnp.einsum('rke,heqw->rqhkw', row_hot, col_table, precision=lax.Precision...  9.27 us
    reduce_scatter x1, waiting for transfers between devices, on_device(): lax.psum_scatter(jnp.dot(attended, w_out, preferred_element_type=jnp.floa...  7.12 us
    dot_general x1, matrix products, on_device(): jnp.einsum('rke,heqw->rqhkw', row_hot, col_table, precision=lax.Precision...  5.61 us
  transfers between devices with their start and end apart: 5, of which 4 were waited for; matrix products, arithmetic and copies ran while one was open for 24% of the time, Pallas kernels for 0%

commit v1 on v0

--- a/solution.py
+++ b/solution.py
@@ -84,11 +84,11 @@
     mod_vecs = lax.psum(placed, ("sp", "tp"))
     normed = rms_mod(latent, norm_gain, mod_vecs[0], mod_vecs[2])
     projected = project(lax.all_gather(normed, "tp", axis=0, tiled=True), (w_query, w_key, w_value))
-    ctx_kv = lax.all_gather(
-        project(rms_mod(context, norm_gain, mod_vecs[1], mod_vecs[3]), (w_key, w_value)),
-        "sp",
+    ctx_kv = jnp.concatenate(
+        lax.all_gather(
+            project(rms_mod(context, norm_gain, mod_vecs[1], mod_vecs[3]), (w_key, w_value)), "sp"
+        ),
         axis=1,
-        tiled=True,
     )
     ctx_key3 = ctx_kv[0].reshape(-1, head_dev, HEAD_DIM)
     ctx_val3 = ctx_kv[1].reshape(-1, head_dev, HEAD_DIM)

time: 194 us -> 194 us (level)
    unnamed x36 -> x35, local copies, waits for them, and re-layouts: 11.5 us -> 8.27 us
    all_gather x0 -> x1, local copies, waits for them, and re-layouts: none -> 2.7 us  [on_device(): lax.all_gather(project(rms_mod(context, norm_gain, mod_vecs[1], mod_vecs[...]
where the time goes in v1:
time: 194 us
  waiting for transfers between devices  53.2 us (27%)
  blocking collectives  42.3 us (22%)
  matrix products  35.6 us (18%)
  local copies, waits for them, and re-layouts  30 us (15%)
  between operations  13.6 us (7%)
  other arithmetic  13.3 us (7%)
  starting transfers between devices  5.61 us (3%)
    psum x1, blocking collectives, on_device(): mod_vecs = lax.psum(placed, ('sp', 'tp'))  42.3 us
    ppermute x1, waiting for transfers between devices, padded_2(): lax.ppermute(tail, axis, [(i, (i + 1) % count) for i in range(ends)])  25.3 us
    all_gather x1, waiting for transfers between devices, on_device(): lax.all_gather(project(rms_mod(context, norm_gain, mod_vecs[1], mod_vecs[...  18.8 us
    dot_general x5, matrix products, project(): jnp.dot(block, weight, preferred_element_type=jnp.float32)  10.6 us
    dot_general x1, local copies, waits for them, and re-layouts, on_device(): jnp.einsum('rke,heqw->rqhkw', row_hot, col_table, precision=lax.Precision...  9.27 us
    unnamed x35, local copies, waits for them, and re-layouts  8.27 us
    reduce_scatter x1, waiting for transfers between devices, on_device(): lax.psum_scatter(jnp.dot(attended, w_out, preferred_element_type=jnp.floa...  7.15 us
    dot_general x1, matrix products, on_device(): jnp.einsum('rke,heqw->rqhkw', row_hot, col_table, precision=lax.Precision...  5.61 us
  transfers between devices with their start and end apart: 5, of which 4 were waited for; matrix products, arithmetic and copies ran while one was open for 24% of the time, Pallas kernels for 0%

profile of v1, /device:TPU:0, one launch (start us, length us, event | category | flops | bytes accessed | tf_op | source)
XLA Modules:
  0.0 193.6 jit_solution(11379791784770473871)
XLA Ops:
  9.9 42.3 %psum.7 = f32[5,2048]{1,0:T(8,128)S(1)} all-reduce(f32[5,2048]{1,0:T(8,128)S(1)} %maximum_dynamic-update-slice_fusion), channel_id=1, replica_groups=mesh['sp'=16,'tp'=2] {'sp','tp'}, use_global_device_ids=true, to_apply=%region_0.1 | all-reduce | flops 10240 | bytes 81920 | tf_op jit(solution)/shard_map/psum | solution.py:84
  53.5 2.1 %fusion.39 = bf16[128,2048]{1,0:T(8,128)(2,1)} fusion(bf16[128,2048]{1,0:T(8,128)(2,1)} %param.13, f32[2048]{0:T(1024)S(1)} %bitcast.163, f32[2048]{0:T(1024)S(1)} %bitcast.164, f32[2048]{0:T(1024)} %param.17, f32[128]{0:T(128)S(1)} %add_rsqrt_fusion.1), kind=kLoop, calls=%fused_computation.45 | loop fusion | flops 1572864 | bytes 1073664 | tf_op jit(solution)/shard_map/convert_element_type | solution.py:37
  57.0 3.2 %fusion.33 = bf16[1,64,1024]{2,1,0:T(8,128)(2,1)S(1)} fusion(bf16[2048,1024]{1,0:T(8,128)(2,1)} %param.22, bf16[64,2048]{1,0:T(8,128)(2,1)} %param.14, f32[2048]{0:T(1024)S(1)} %bitcast.158, f32[2048]{0:T(1024)S(1)} %bitcast.160, f32[2048]{0:T(1024)} %param.17, f32[64]{0:T(128)S(1)} %add_rsqrt_fusion), kind=kOutput, calls=%fused_computation.39 | convolution fusion | flops 269287424 | bytes 4612352 | tf_op jit(solution)/shard_map/dot_general | solution.py:43
  62.1 1.4 fusion.51
  63.5 5.6 %fusion.12 = f32[8,32,32,8,8]{2,4,3,1,0:T(8,128)} fusion(f32[8,15,32,32]{3,1,2,0:T(8,128)S(1)} %fusion.51, s32[8,8]{1,0:T(8,128)S(1)} %subtract_add_fusion), kind=kOutput, calls=%fused_computation.20 | convolution fusion | flops 94372800 | bytes 2588928 | tf_op jit(solution)/shard_map/rke,heqw->rqhkw/dot_general | solution.py:132
  69.2 9.3 %copy.59 = f32[8,32,32,8,8]{1,2,4,0,3:T(8,128)} copy(f32[8,32,32,8,8]{2,4,3,1,0:T(8,128)} %fusion.12) | data formatting | bytes 4194304 | tf_op jit(solution)/shard_map/rke,heqw->rqhkw/dot_general | solution.py:132
  78.5 3.9 %convolution_convert_fusion.2 = bf16[256,1024]{1,0:T(8,128)(2,1)S(1)} fusion(bf16[256,2048]{1,0:T(8,128)(2,1)} %all-gather.4.cloned.1.call-done, bf16[2048,1024]{1,0:T(8,128)(2,1)} %param.23), kind=kOutput, calls=%fused_computation.34 | convolution fusion | flops 1074003968 | bytes 5767168 | tf_op jit(solution)/shard_map/dot_general | solution.py:43
  83.9 4.2 %collective-permute-start = (bf16[2,4,32,1024]{3,2,0,1:T(8,128)(2,1)S(1)}, bf16[2,4,32,1024]{3,2,0,1:T(8,128)(2,1)S(1)}, u32[]{:S(2)}, u32[]{:S(2)}) collective-permute-start(bf16[2,4,32,1024]{3,2,0,1:T(8,128)(2,1)S(1)} %get-tuple-element.9), channel_id=1, source_target_pairs={{0,2},{2,4},{4,6},{6,8},{8,10},{10,12},{12,14},{14,16},{16,18},{18... | collective-permute-start | bytes 1572872 | tf_op jit(solution)/shard_map/ppermute | solution.py:23
  88.2 1.3 collective-permute-start.1
  91.0 25.3 %collective-permute-done = bf16[2,4,32,1024]{3,2,0,1:T(8,128)(2,1)S(1)} collective-permute-done((bf16[2,4,32,1024]{3,2,0,1:T(8,128)(2,1)S(1)}, bf16[2,4,32,1024]{3,2,0,1:T(8,128)(2,1)S(1)}, u32[]{:S(2)}, u32[]{:S(2)}) %collective-permute-start) | collective-permute-done | bytes 524320 | tf_op jit(solution)/shard_map/ppermute | solution.py:23
  116.3 1.9 collective-permute-done.1
  118.5 4.9 %gather_fusion = bf16[8,2,8,32,1024]{4,3,1,2,0:T(8,128)(2,1)} fusion(bf16[2,16,32,1024]{3,2,0,1:T(8,128)(2,1)S(1)} %pad_maximum_fusion, s32[8]{0:T(128)S(1)} %shift-left_bitcast_fusion), kind=kCustom, calls=%fused_computation | custom fusion | bytes 16777344 | tf_op jit(solution)/shard_map/vmap()/gather | solution.py:109
  123.4 4.0 %fusion.66 = (bf16[8,1,8,32,1024]{4,3,1,2,0:T(8,128)(2,1)S(1)}, bf16[8,1,8,32,1024]{4,3,1,2,0:T(8,128)(2,1)S(1)}) fusion(bf16[8,2,8,32,1024]{4,3,1,2,0:T(8,128)(2,1)} %gather_fusion), kind=kLoop, calls=%fused_computation.98 | loop fusion | bytes 16777216 | tf_op jit(solution)/shard_map/slice | solution.py:113
  128.5 3.3 %copy.81 = bf16[256,8,8,128]{3,2,1,0:T(8,128)(2,1)} copy(bf16[256,8,8,128]{3,1,2,0:T(8,128)(2,1)S(1)} %bitcast.142) | data formatting | bytes 8388608
  133.0 4.3 %fusion.69 = (f32[8,32,8]{1,2,0:T(8,128)S(1)}, f32[8,32,8,8,32]{1,4,3,2,0:T(8,128)}) fusion(f32[8,32,32,8,8]{1,2,4,0,3:T(8,128)S(1)} %bitcast.137, bf16[8,32,8,128,1]{3,2,1,0,4:T(8,128)(2,1)S(1)} %bitcast_bitcast_fusion, bf16[8,8,32,8,128]{4,3,2,1,0:T(8,128)(2,1)S(1)} %bitcast.141, pred[32,32]{0,1:T(8,128)(4,1)S(1)} %fusion.57), kind=kOutput, calls=%fused_computation.101 | convolution fusion | flops 136312832 | bytes 8922112 | tf_op jit(solution)/shard_map/rqhd,rkwhd->rqhkw/dot_general | solution.py:135
  137.3 18.8 %all-gather.6.cloned.1.call-done = bf16[32,64,1024]{2,1,0:T(8,128)(2,1)} async-done(((bf16[2,64,1024]{2,1,0:T(8,128)(2,1)}), bf16[32,64,1024]{2,1,0:T(8,128)(2,1)}) %all-gather.6.cloned.1.call-update) | async-done | bytes 4194320 | tf_op jit(solution)/shard_map/all_gather | solution.py:88
  156.1 2.7 %copy.126 = bf16[16,2,64,1024]{3,2,0,1:T(8,128)(2,1)S(1)} copy(bf16[16,2,64,1024]{3,2,1,0:T(8,128)(2,1)} %bitcast.149) | data formatting | bytes 8388608 | tf_op jit(solution)/shard_map/all_gather | solution.py:88
  162.0 1.9 fusion.3
  164.9 2.0 %fusion.2 = f32[8,32,8]{1,2,0:T(8,128)S(1)} fusion(f32[8,32,8,8,32]{1,4,3,2,0:T(8,128)S(1)} %bitcast.139, f32[8,32,8]{1,2,0:T(8,128)S(1)} %copy_maximum_fusion), kind=kLoop, calls=%fused_computation.9 | loop fusion | flops 1046528 | bytes 2113536 | tf_op jit(solution)/shard_map/reduce_sum | solution.py:148
  167.6 3.3 %fusion.21 = f32[8,32,8,128]{3,1,2,0:T(8,128)S(1)} fusion(bf16[1024,8,128]{2,1,0:T(8,128)(2,1)S(1)} %bitcast.151, f32[8,32,8]{1,0,2:T(8,128)S(1)} %copy.68, f32[8,32,8]{1,0,2:T(8,128)S(1)} %copy.64, f32[8,1024,256]{1,2,0:S(1)} %fusion.16), kind=kOutput, calls=%fused_computation.30 | convolution fusion | flops 545259520 | bytes 11550720 | tf_op jit(solution)/shard_map/rqhc,chd->rqhd/dot_general | solution.py:155
  170.9 2.3 %fusion.29 = bf16[8,32,8,128]{3,1,2,0:T(8,128)(2,1)S(1)} fusion(f32[8,32,8,128]{3,1,2,0:T(8,128)S(1)} %fusion.21, f32[8,32,8,8,32]{1,4,3,2,0:T(8,128)S(1)} %bitcast.139, f32[8,32,8]{1,2,0:T(8,128)S(1)} %copy_add_fusion, f32[8,32,8]{1,2,0:T(8,128)S(1)} %copy_maximum_fusion, bf16[8,8,32,8,128]{4,3,2,1,0:T(8,128)(2,1)S(1)} %bitcast.150), kind=kOutput, calls=%fused_computation.32 | convolution fusion | flops 136314880 | bytes 7880704 | tf_op jit(solution)/shard_map/rqhkw,rkwhd->rqhd/dot_general | solution.py:152
  173.4 4.5 %convolution_convert_fusion = bf16[256,2048]{1,0:T(8,128)(2,1)} fusion(bf16[1024,2048]{1,0:T(8,128)(2,1)} %param.24, bf16[32,8,8,128]{3,2,1,0:T(8,128)(2,1)S(1)} %bitcast.157), kind=kOutput, calls=%fused_computation.18 | convolution fusion | flops 1074266112 | bytes 5767168 | tf_op jit(solution)/shard_map/dot_general | solution.py:160
  177.9 7.2 %reduce-scatter.2.cloned.1.call-done = bf16[128,2048]{1,0:T(8,128)(2,1)} async-done(((bf16[256,2048]{1,0:T(8,128)(2,1)}), bf16[128,2048]{1,0:T(8,128)(2,1)}) %reduce-scatter.2.cloned.1.call-update) | async-done | bytes 524304 | tf_op jit(solution)/shard_map/reduce_scatter | solution.py:159
  185.1 2.0 %fusion.40 = bf16[128,2048]{1,0:T(8,128)(2,1)} fusion(bf16[128,2048]{1,0:T(8,128)(2,1)S(1)} %copy-done.2, bf16[128,2048]{1,0:T(8,128)(2,1)} %reduce-scatter.2.cloned.1.call-done, f32[2048]{0:T(1024)S(1)} %bitcast.162), kind=kLoop, calls=%fused_computation.46 | loop fusion | flops 1310720 | bytes 1581056 | tf_op jit(solution)/shard_map/convert_element_type | solution.py:165
  (77 shorter events, 18.4 us)
Async XLA Ops:
  6.5 1.0 copy-start
  6.5 53.7 %copy-start.7 = (f32[2048]{0:T(1024)S(1)}, f32[2048]{0:T(1024)}, u32[]{:S(2)}) copy-start(f32[2048]{0:T(1024)} %param.17) | copy-start | bytes 24580
  6.5 53.7 %copy-start.6 = (bf16[64,2048]{1,0:T(8,128)(2,1)S(1)}, bf16[64,2048]{1,0:T(8,128)(2,1)}, u32[]{:S(2)}) copy-start(bf16[64,2048]{1,0:T(8,128)(2,1)} %param.14) | copy-start | bytes 786436
  6.5 72.0 %all-gather.4.cloned.1.call-start = ((), (), s32[]{:S(2)}) async-start(), calls=%async_computation.1 | async-start | bytes 1572864 | tf_op jit(solution)/shard_map/all_gather | solution.py:86
  55.6 100.5 %all-gather.6.cloned.1.call-start = ((), (), s32[]{:S(2)}) async-start(), calls=%async_computation.3 | async-start | bytes 4456448 | tf_op jit(solution)/shard_map/all_gather | solution.py:88
  55.7 4.6 %copy-start.3 = (bf16[2048,1024]{1,0:T(8,128)(2,1)S(1)}, bf16[2048,1024]{1,0:T(8,128)(2,1)}, u32[]{:S(2)}) copy-start(bf16[2048,1024]{1,0:T(8,128)(2,1)} %param.23) | copy-start | bytes 12582916
  56.9 5.0 %copy-start.8 = (f32[16,15,31]{2,0,1:T(8,128)S(1)}, f32[16,15,31]{2,0,1:T(8,128)}, u32[]{:S(2)}) copy-start(f32[16,15,31]{2,0,1:T(8,128)} %param.25) | copy-start | bytes 89284
  61.9 123.2 %reduce-scatter.2.cloned.1.call-start = ((), (), s32[]{:S(2)}) async-start(), calls=%async_computation.2 | async-start | bytes 1572864 | tf_op jit(solution)/shard_map/reduce_scatter | solution.py:159
  78.5 3.9 %copy-start.4 = (bf16[2048,1024]{1,0:T(8,128)(2,1)S(1)}, bf16[2048,1024]{1,0:T(8,128)(2,1)}, u32[]{:S(2)}) copy-start(bf16[2048,1024]{1,0:T(8,128)(2,1)} %param.22) | copy-start | bytes 12582916
  78.5 4.0 %copy-start.10 = (bf16[256,2048]{1,0:T(8,128)(2,1)S(1)}, bf16[256,2048]{1,0:T(8,128)(2,1)}, u32[]{:S(2)}) copy-start(bf16[256,2048]{1,0:T(8,128)(2,1)} %all-gather.4.cloned.1.call-done) | copy-start | bytes 3145732
  82.6 6.9 %copy-start.9 = (bf16[2048,1024]{1,0:T(8,128)(2,1)S(1)}, bf16[2048,1024]{1,0:T(8,128)(2,1)}, u32[]{:S(2)}) copy-start(bf16[2048,1024]{1,0:T(8,128)(2,1)} %param.21) | copy-start | bytes 12582916
  83.9 32.4 %collective-permute-start = (bf16[2,4,32,1024]{3,2,0,1:T(8,128)(2,1)S(1)}, bf16[2,4,32,1024]{3,2,0,1:T(8,128)(2,1)S(1)}, u32[]{:S(2)}, u32[]{:S(2)}) collective-permute-start(bf16[2,4,32,1024]{3,2,0,1:T(8,128)(2,1)S(1)} %get-tuple-element.9), channel_id=1, source_target_pairs={{0,2},{2,4},{4,6},{6,8},{8,10},{10,12},{12,14},{14,16},{16,18},{18... | collective-permute-start | bytes 1572872 | tf_op jit(solution)/shard_map/ppermute | solution.py:23
  88.2 30.0 %collective-permute-start.1 = (bf16[2,4,32,1024]{3,2,0,1:T(8,128)(2,1)S(1)}, bf16[2,4,32,1024]{3,2,0,1:T(8,128)(2,1)S(1)}, u32[]{:S(2)}, u32[]{:S(2)}) collective-permute-start(bf16[2,4,32,1024]{3,2,0,1:T(8,128)(2,1)S(1)} %get-tuple-element.10), channel_id=1, source_target_pairs={{2,0},{4,2},{6,4},{8,6},{10,8},{12,10},{14,12},{16,14},{18,16},{20... | collective-permute-start | bytes 1572872 | tf_op jit(solution)/shard_map/ppermute | solution.py:25
  127.3 4.5 %slice-start = ((s8[8388608]{0:T(1024)(128)(4,1)}), s8[4194304]{0:T(1024)(128)(4,1)S(1)}, s32[]{:S(2)}) async-start(s8[8388608]{0:T(1024)(128)(4,1)} %bitcast.136), calls=%async_computation.4 | async-start | bytes 8388608
  128.5 4.5 %slice-start.1 = ((s8[8388608]{0:T(1024)(128)(4,1)}), s8[4194304]{0:T(1024)(128)(4,1)S(1)}, s32[]{:S(2)}) async-start(s8[8388608]{0:T(1024)(128)(4,1)} %bitcast.136), calls=%async_computation.5 | async-start | bytes 8388608
  161.2 2.6 %slice-start.2 = ((s8[8388608]{0:T(1024)(128)(4,1)}), s8[4194304]{0:T(1024)(128)(4,1)S(1)}, s32[]{:S(2)}) async-start(s8[8388608]{0:T(1024)(128)(4,1)} %bitcast.138), calls=%async_computation.6 | async-start | bytes 8388608
  162.0 2.9 %slice-start.3 = ((s8[8388608]{0:T(1024)(128)(4,1)}), s8[4194304]{0:T(1024)(128)(4,1)S(1)}, s32[]{:S(2)}) async-start(s8[8388608]{0:T(1024)(128)(4,1)} %bitcast.138), calls=%async_computation.7 | async-start | bytes 8388608
  167.6 3.3 %copy-start.5 = (bf16[256,8,8,128]{3,2,1,0:T(8,128)(2,1)S(1)}, bf16[256,8,8,128]{3,2,1,0:T(8,128)(2,1)}, u32[]{:S(2)}) copy-start(bf16[256,8,8,128]{3,2,1,0:T(8,128)(2,1)} %copy.81) | copy-start | bytes 12582916
  173.4 11.7 %copy-start.2 = (bf16[128,2048]{1,0:T(8,128)(2,1)S(1)}, bf16[128,2048]{1,0:T(8,128)(2,1)}, u32[]{:S(2)}) copy-start(bf16[128,2048]{1,0:T(8,128)(2,1)} %param.13) | copy-start | bytes 1572868
  173.4 13.7 %copy-start.1 = (bf16[128,1024]{1,0:T(8,128)(2,1)S(1)}, bf16[128,1024]{1,0:T(8,128)(2,1)}, u32[]{:S(2)}) copy-start(bf16[128,1024]{1,0:T(8,128)(2,1)} %param.18) | copy-start | bytes 786436
Sparse Core Ops, SparseCore 0:
  55.7 8.8 all-gather.3
  67.4 88.6 all-gather.5
  178.1 6.9 reduce-scatter.1
